TPU v7x, 32 devices: a whole 2x2x4 slice. The times are simulated.
32 devices in a mesh: sp: 4 (over z), tp: 8 (over y, x, core).
Axes of the slice: x: 2, y: 2, z: 4, core: 2. Of those that a mesh axis runs over, the one named last changes fastest.
Arguments:
- activations: bfloat16 [1024, 2048], P('sp', 'tp'), may hold values from -170 to 170
- norm_gain: float32 [2048], replicated, may hold values from 0.1 to 1.9
- query_weight: bfloat16 [2048, 1536], P(None, 'tp'), may hold values from -0.125 to 0.125
- latent_weight: bfloat16 [2048, 512], P(None, 'tp'), may hold values from -0.125 to 0.125
- rope_key_weight: bfloat16 [2048, 64], replicated, may hold values from -0.125 to 0.125
- latent_gain: float32 [512], replicated, may hold values from 1.5 to 64
- expand_weight: bfloat16 [512, 2048], P(None, 'tp'), may hold values from -0.25 to 0.25
- gate_weight: bfloat16 [2048, 1024], P(None, 'tp'), may hold values from -0.125 to 0.125
- pre_weight: bfloat16 [2048, 1024], P(None, 'tp'), may hold values from -0.125 to 0.125
- value_weight: bfloat16 [2048, 1024], P(None, 'tp'), may hold values from -0.125 to 0.125
- conv_kernel: bfloat16 [3, 1024], P(None, 'tp'), may hold values from -3.5 to 3.5
- output_attend: bfloat16 [1024, 2048], P('tp'), may hold values from -0.1875 to 0.1875
- output_conv: bfloat16 [1024, 2048], P('tp'), may hold values from -0.125 to 0.125
Outputs:
- mixed: bfloat16 [1024, 2048], P(('sp', 'tp'))
- log_weight_sum: float32 [8, 1024], P('tp', 'sp')
All inputs are finite; a program needn't handle non-finite values.
Results may differ from a plain program's by a relative error of at most 0.035.
The roundings to bfloat16 on the way count: a program that leaves them out, or rounds other values in their place, can miss the bound.
Values may be sent and summed in bfloat16 or wider, within the bound.
A program may use at most 128 MiB of HBM per device.

v0:
```python
import math
import jax
import jax.numpy as jnp
from jax import lax
from jax.sharding import PartitionSpec as P

D = 2048
NOPE = 128
ROPE = 64
VDIM = 128
GRID_W = 64
EPSILON = 1e-06
ROPE_BASE = 10000.0


def with_halo(array, sides, width):
    for axis, dim in sides:
        peers, length = (lax.axis_size(axis), array.shape[dim])
        up = [(i, (i + 1) % peers) for i in range(peers - 1)]
        down = [(j, i) for i, j in up]
        last = lax.slice_in_dim(array, length - width, length, axis=dim)
        leading = lax.slice_in_dim(array, 0, width, axis=dim)
        before = lax.ppermute(last, axis, up)
        after = lax.ppermute(leading, axis, down)
        array = jnp.concatenate([before, array, after], axis=dim)
    return array


def rotate(inputs, grid_rows, grid_cols):
    quarter = inputs.shape[-1] // 4
    inverse = ROPE_BASE ** (-jnp.arange(quarter, dtype=jnp.float32) / quarter)
    row_angle = (grid_rows[:, None] * inverse)[:, None, :]
    col_angle = (grid_cols[:, None] * inverse)[:, None, :]
    part_one = inputs[..., :quarter]
    part_two = inputs[..., quarter : 2 * quarter]
    part_three = inputs[..., 2 * quarter : 3 * quarter]
    part_four = inputs[..., 3 * quarter :]
    return jnp.concatenate(
        [
            part_one * jnp.cos(row_angle) - part_two * jnp.sin(row_angle),
            part_one * jnp.sin(row_angle) + part_two * jnp.cos(row_angle),
            part_three * jnp.cos(col_angle) - part_four * jnp.sin(col_angle),
            part_three * jnp.sin(col_angle) + part_four * jnp.cos(col_angle),
        ],
        axis=-1,
    )


def conv_branch(gate_proj, pre_proj, value_proj, conv_kernel):
    pre_mix = (pre_proj * value_proj).astype(jnp.bfloat16)
    padded = with_halo(pre_mix, (("sp", 0),), 1).astype(jnp.float32)
    kernel = conv_kernel.astype(jnp.float32)
    convolved = kernel[0] * padded[:-2] + kernel[1] * padded[1:-1] + kernel[2] * padded[2:]
    return (gate_proj * convolved).astype(jnp.bfloat16)


def body(
    activations,
    norm_gain,
    query_weight,
    latent_weight,
    rope_key_weight,
    latent_gain,
    expand_weight,
    gate_weight,
    pre_weight,
    value_weight,
    conv_kernel,
    output_attend,
    output_conv,
):
    tokens_here = activations.shape[0]
    query_cols = query_weight.shape[1]
    heads_here = query_cols // (NOPE + ROPE)
    latent_cols = latent_weight.shape[1]
    channels = gate_weight.shape[1]
    joined = jnp.concatenate(
        [query_weight, latent_weight, rope_key_weight, gate_weight, pre_weight, value_weight],
        axis=1,
    )
    inputs_f32 = activations.astype(jnp.float32)
    squares = lax.psum(jnp.sum(inputs_f32 * inputs_f32, axis=1, keepdims=True), "tp")
    partial_squares = jnp.zeros((tokens_here, 1), jnp.float32)
    piece_f32 = lax.all_gather(activations, "tp", axis=1, tiled=True).astype(jnp.float32)
    scaled = (piece_f32 * norm_gain).astype(jnp.bfloat16)
    running = jnp.dot(scaled, joined, preferred_element_type=jnp.float32)
    running, folded_squares = (running, partial_squares)
    inv_rms = lax.rsqrt(squares / D + EPSILON)
    projected = running * inv_rms
    latent_end = query_cols + latent_cols
    rope_end = latent_end + ROPE
    query_proj = projected[:, :query_cols]
    latent_proj = projected[:, query_cols:latent_end]
    rope_proj = projected[:, latent_end:rope_end]
    gate_proj = projected[:, rope_end : rope_end + channels]
    pre_proj = projected[:, rope_end + channels : rope_end + 2 * channels]
    value_proj = projected[:, rope_end + 2 * channels :]
    positions = lax.axis_index("sp") * tokens_here + jnp.arange(tokens_here, dtype=jnp.int32)
    grid_rows = (positions // GRID_W).astype(jnp.float32)
    grid_cols = (positions % GRID_W).astype(jnp.float32)
    query = query_proj.reshape(tokens_here, heads_here, NOPE + ROPE)
    query = jnp.concatenate(
        [query[..., :NOPE], rotate(query[..., NOPE:], grid_rows, grid_cols)], axis=-1
    )
    query = (query * (NOPE + ROPE) ** (-0.5)).astype(jnp.bfloat16)
    query_nope = query[..., :NOPE]
    query_rope = query[..., NOPE:]
    gathered = lax.all_gather(latent_proj.astype(jnp.bfloat16), "tp", axis=1, tiled=True).astype(
        jnp.float32
    )
    latent = (
        gathered
        * lax.rsqrt(jnp.mean(gathered * gathered, axis=1, keepdims=True) + EPSILON)
        * latent_gain
    ).astype(jnp.bfloat16)
    expanded = jnp.dot(latent, expand_weight, preferred_element_type=jnp.float32).astype(
        jnp.bfloat16
    )
    rope_key = rotate(rope_proj[:, None, :], grid_rows, grid_cols)[:, 0].astype(jnp.bfloat16)
    starting = (
        jnp.full((heads_here, tokens_here), -jnp.inf, jnp.float32),
        jnp.zeros((heads_here, tokens_here), jnp.float32),
        jnp.zeros((tokens_here, heads_here, VDIM), jnp.float32),
    )
    key_piece = lax.all_gather(expanded, "sp", axis=0, tiled=True)
    rope_piece = lax.all_gather(rope_key, "sp", axis=0, tiled=True)
    piece_rows = key_piece.shape[0]
    key_block = math.gcd(piece_rows, 1024)
    split_heads = key_piece.reshape(piece_rows, heads_here, NOPE + VDIM)

    def one_block(turn_index, state):
        row_max, row_sum, running_out = state
        offset = turn_index * key_block
        block_keys = lax.dynamic_slice_in_dim(split_heads, offset, key_block, 0)
        block_rope = lax.dynamic_slice_in_dim(rope_piece, offset, key_block, 0)
        scores = jnp.einsum(
            "thd,jhd->htj", query_nope, block_keys[..., :NOPE], preferred_element_type=jnp.float32
        )
        scores = scores + jnp.einsum(
            "thd,jd->htj", query_rope, block_rope, preferred_element_type=jnp.float32
        )
        new_max = jnp.maximum(row_max, jnp.max(scores, axis=-1))
        rescale = jnp.exp(row_max - new_max)
        weights = jnp.exp(scores - new_max[..., None])
        row_sum = row_sum * rescale + jnp.sum(weights, axis=-1)
        running_out = running_out * rescale.T[..., None] + jnp.einsum(
            "htj,jhd->thd",
            weights.astype(jnp.bfloat16),
            block_keys[..., NOPE:],
            preferred_element_type=jnp.float32,
        )
        return (new_max, row_sum, running_out)

    row_max, row_sum, running_out = lax.fori_loop(0, piece_rows // key_block, one_block, starting)
    attended = (
        (running_out / row_sum.T[..., None])
        .astype(jnp.bfloat16)
        .reshape(tokens_here, heads_here * VDIM)
    )
    log_weight_sum = row_max + jnp.log(row_sum)
    conv_mixed = conv_branch(gate_proj, pre_proj, value_proj, conv_kernel)
    mixed = lax.psum_scatter(
        (
            jnp.dot(attended, output_attend, preferred_element_type=jnp.float32)
            + jnp.dot(conv_mixed, output_conv, preferred_element_type=jnp.float32)
        ).astype(jnp.bfloat16),
        "tp",
        scatter_dimension=0,
        tiled=True,
    )
    return (mixed, log_weight_sum)


def solution(mesh):
    return jax.shard_map(
        body,
        mesh=mesh,
        in_specs=(
            P("sp", "tp"),
            P(),
            P(None, "tp"),
            P(None, "tp"),
            P(),
            P(),
            P(None, "tp"),
            P(None, "tp"),
            P(None, "tp"),
            P(None, "tp"),
            P(None, "tp"),
            P("tp", None),
            P("tp", None),
        ),
        out_specs=(P(("sp", "tp"), None), P("tp", "sp")),
        check_vma=False,
    )
```

profile of v0, /device:TPU:0, one launch (start us, length us, event | category | flops | bytes accessed | tf_op | source)
XLA Modules:
  0.0 135.6 jit_solution(17453811287171782455)
XLA Ops:
  7.3 0.7 all-gather.3.cloned.1.call-update
  8.0 1.0 multiply_reduce_fusion
  9.0 1.2 copy.19
  10.3 1.3 copy.20
  11.5 1.2 copy.21
  12.8 15.2 %psum.7 = f32[256,1]{0,1:T(1,128)S(1)} all-reduce(f32[256,1]{0,1:T(1,128)S(1)} %bitcast.73), channel_id=1, replica_groups=mesh['sp'=4,'tp'=8] {'tp'}, use_global_device_ids=true, to_apply=%region_1.0 | all-reduce | flops 256 | bytes 2048 | tf_op jit(solution)/shard_map/psum | solution.py:82
  28.0 0.6 slice_bitcast_fusion.13
  28.6 0.9 constant_dynamic-update-slice_fusion.5
  29.6 0.7 constant_dynamic-update-slice_fusion.4
  30.3 0.7 constant_dynamic-update-slice_fusion.3
  31.0 0.8 constant_dynamic-update-slice_fusion.2
  31.8 0.9 constant_dynamic-update-slice_fusion.1
  32.7 0.8 constant_dynamic-update-slice_fusion
  33.5 2.7 %all-gather.3.cloned.1.call-done = bf16[256,2048]{1,0:T(8,128)(2,1)} async-done(((bf16[256,256]{1,0:T(8,128)(2,1)}), bf16[256,2048]{1,0:T(8,128)(2,1)}) %all-gather.3.cloned.1.call-update) | async-done | bytes 1048592 | tf_op jit(solution)/shard_map/all_gather | solution.py:84
  36.2 3.1 %convolution_multiply_fusion = f32[256,704]{0,1:T(8,128)S(1)} fusion(bf16[2048,704]{0,1:T(8,128)(2,1)} %constant_dynamic-update-slice_fusion, bf16[256,2048]{1,0:T(8,128)(2,1)} %all-gather.3.cloned.1.call-done, f32[2048]{0:T(1024)S(1)} %copy-done.7, f32[256]{0:T(256)S(1)} %bitcast.74), kind=kOutput, calls=%fused_computation.6 | convolution fusion | flops 739950592 | bytes 4662272 | tf_op jit(solution)/shard_map/dot_general | solution.py:86
  39.9 13.4 %all-gather = bf16[1024,1,64]{0,2,1:T(8,128)(2,1)S(1)} all-gather(bf16[256,1,64]{0,2,1:T(8,128)(2,1)S(1)} %pad_maximum_fusion), channel_id=2, replica_groups=mesh['sp'=4,'tp'=8] {'sp'}, dimensions={0}, use_global_device_ids=true | all-gather | bytes 163840 | tf_op jit(solution)/shard_map/all_gather | solution.py:126
  53.5 9.3 %all_gather.13 = bf16[256,512]{0,1:T(8,128)(2,1)S(1)} all-gather(bf16[256,64]{0,1:T(8,128)(2,1)S(1)} %slice.196), channel_id=1, replica_groups=mesh['sp'=4,'tp'=8] {'tp'}, dimensions={1}, use_global_device_ids=true | all-gather | bytes 294912 | tf_op jit(solution)/shard_map/all_gather | solution.py:108
  63.3 16.1 %all_gather.14 = bf16[1024,256]{1,0:T(8,128)(2,1)S(1)} all-gather(bf16[256,256]{1,0:T(8,128)(2,1)S(1)} %convolution_convert_fusion), channel_id=1, replica_groups=mesh['sp'=4,'tp'=8] {'sp'}, dimensions={0}, use_global_device_ids=true | all-gather | bytes 655360 | tf_op jit(solution)/shard_map/all_gather | solution.py:125
  80.5 3.7 %collective-permute-start = (bf16[1,128]{0,1:T(8,128)(2,1)S(1)}, bf16[1,128]{0,1:T(8,128)(2,1)S(1)}, u32[]{:S(2)}, u32[]{:S(2)}) collective-permute-start(bf16[1,128]{0,1:T(8,128)(2,1)S(1)} %get-tuple-element.26), channel_id=1, source_target_pairs={{0,8},{8,16},{16,24},{1,9},{9,17},{17,25},{2,10},{10,18},{18,26},{... | collective-permute-start | bytes 776 | tf_op jit(solution)/shard_map/ppermute | solution.py:23
  84.2 1.3 collective-permute-start.1
  85.5 2.4 %fusion.9 = f32[256,2048]{1,0:T(8,128)} fusion(bf16[128,2048]{1,0:T(8,128)(2,1)S(1)} %copy-done, f32[1,256,1024]{2,1,0:T(8,128)S(1)} %get-tuple-element.44, f32[256]{0:T(256)S(1)} %get-tuple-element.43, bf16[1024,1,256]{2,0,1:T(8,128)(2,1)S(1)} %bitcast.70, f32[256]{0:T(256)S(1)} %get-tuple-element.42, f32[256]{0:T(256)S(1)} %get-tuple-element.41), kind=kOutput, calls=%fused_computation.19 | convolution fusion | flops 201949184 | bytes 3935232 | tf_op jit(solution)/shard_map/dot_general | solution.py:164
  88.0 2.1 %collective-permute-done.1 = bf16[1,128]{0,1:T(8,128)(2,1)S(1)} collective-permute-done((bf16[1,128]{0,1:T(8,128)(2,1)S(1)}, bf16[1,128]{0,1:T(8,128)(2,1)S(1)}, u32[]{:S(2)}, u32[]{:S(2)}) %collective-permute-start.1) | collective-permute-done | bytes 288 | tf_op jit(solution)/shard_map/ppermute | solution.py:24
  90.2 3.2 %fusion = bf16[256,2048]{1,0:T(8,128)(2,1)} fusion(f32[256,2048]{1,0:T(8,128)} %fusion.9, bf16[128,2048]{1,0:T(8,128)(2,1)S(1)} %copy-done.2, f32[258,128]{0,1:T(8,128)S(1)} %maximum_convert_fusion, f32[256,704]{0,1:T(8,128)S(1)} %convolution_multiply_fusion, f32[128]{0:T(128)} %get-tuple-element.38, f32[128]{0:T(128)} %get-tuple-element.39, ...), kind=kOutput, calls=%fused_computation.1 | convolution fusion | flops 135495680 | bytes 4195840 | tf_op jit(solution)/shard_map/dot_general | solution.py:165
  94.0 34.8 %reduce-scatter.2.cloned.1.call-done = bf16[32,2048]{1,0:T(8,128)(2,1)} async-done(((bf16[256,2048]{1,0:T(8,128)(2,1)}), bf16[32,2048]{1,0:T(8,128)(2,1)}) %reduce-scatter.2.cloned.1.call-update) | async-done | bytes 131088 | tf_op jit(solution)/shard_map/reduce_scatter | solution.py:162
  (47 shorter events, 3.2 us)
Async XLA Ops:
  7.2 78.4 %copy-start = (bf16[128,2048]{1,0:T(8,128)(2,1)S(1)}, bf16[128,2048]{1,0:T(8,128)(2,1)}, u32[]{:S(2)}) copy-start(bf16[128,2048]{1,0:T(8,128)(2,1)} %param.24) | copy-start | bytes 1572868
  7.2 20.8 %copy-start.5 = (bf16[3,128]{1,0:T(4,128)(2,1)S(1)}, bf16[3,128]{1,0:T(4,128)(2,1)}, u32[]{:S(2)}) copy-start(bf16[3,128]{1,0:T(4,128)(2,1)} %param.23) | copy-start | bytes 2308
  7.2 21.4 %copy-start.1 = (bf16[2048,192]{0,1:T(8,128)(2,1)S(1)}, bf16[2048,192]{0,1:T(8,128)(2,1)}, u32[]{:S(2)}) copy-start(bf16[2048,192]{0,1:T(8,128)(2,1)} %param.15) | copy-start | bytes 2359300
  7.2 22.3 %copy-start.3 = (bf16[2048,64]{0,1:T(8,128)(2,1)S(1)}, bf16[2048,64]{0,1:T(8,128)(2,1)}, u32[]{:S(2)}) copy-start(bf16[2048,64]{0,1:T(8,128)(2,1)} %param.16) | copy-start | bytes 786436
  7.2 23.1 %copy-start.4 = (bf16[2048,64]{0,1:T(8,128)(2,1)S(1)}, bf16[2048,64]{0,1:T(8,128)(2,1)}, u32[]{:S(2)}) copy-start(bf16[2048,64]{0,1:T(8,128)(2,1)} %param.17) | copy-start | bytes 786436
  7.2 29.0 %all-gather.3.cloned.1.call-start = ((), (), s32[]{:S(2)}) async-start(), calls=%async_computation.1 | async-start | bytes 1179648 | tf_op jit(solution)/shard_map/all_gather | solution.py:84
  8.0 120.8 %reduce-scatter.2.cloned.1.call-start = ((), (), s32[]{:S(2)}) async-start(), calls=%async_computation.2 | async-start | bytes 1179648 | tf_op jit(solution)/shard_map/reduce_scatter | solution.py:162
  28.6 7.6 %copy-start.7 = (f32[2048]{0:T(1024)S(1)}, f32[2048]{0:T(1024)}, u32[]{:S(2)}) copy-start(f32[2048]{0:T(1024)} %param.14) | copy-start | bytes 24580
  36.2 26.7 %copy-start.6 = (bf16[512,256]{1,0:T(8,128)(2,1)S(1)}, bf16[512,256]{1,0:T(8,128)(2,1)}, u32[]{:S(2)}) copy-start(bf16[512,256]{1,0:T(8,128)(2,1)} %param.19) | copy-start | bytes 786436
  36.2 26.7 %copy-start.8 = (f32[512]{0:T(512)S(1)}, f32[512]{0:T(512)}, u32[]{:S(2)}) copy-start(f32[512]{0:T(512)} %param.18) | copy-start | bytes 6148
  80.1 10.0 %copy-start.2 = (bf16[128,2048]{1,0:T(8,128)(2,1)S(1)}, bf16[128,2048]{1,0:T(8,128)(2,1)}, u32[]{:S(2)}) copy-start(bf16[128,2048]{1,0:T(8,128)(2,1)} %param.25) | copy-start | bytes 1572868
  80.5 7.4 %collective-permute-start = (bf16[1,128]{0,1:T(8,128)(2,1)S(1)}, bf16[1,128]{0,1:T(8,128)(2,1)S(1)}, u32[]{:S(2)}, u32[]{:S(2)}) collective-permute-start(bf16[1,128]{0,1:T(8,128)(2,1)S(1)} %get-tuple-element.26), channel_id=1, source_target_pairs={{0,8},{8,16},{16,24},{1,9},{9,17},{17,25},{2,10},{10,18},{18,26},{... | collective-permute-start | bytes 776 | tf_op jit(solution)/shard_map/ppermute | solution.py:23
  84.2 5.8 %collective-permute-start.1 = (bf16[1,128]{0,1:T(8,128)(2,1)S(1)}, bf16[1,128]{0,1:T(8,128)(2,1)S(1)}, u32[]{:S(2)}, u32[]{:S(2)}) collective-permute-start(bf16[1,128]{0,1:T(8,128)(2,1)S(1)} %get-tuple-element.36), channel_id=1, source_target_pairs={{8,0},{16,8},{24,16},{9,1},{17,9},{25,17},{10,2},{18,10},{26,18},{... | collective-permute-start | bytes 776 | tf_op jit(solution)/shard_map/ppermute | solution.py:24
Sparse Core Ops, SparseCore 0:
  9.9 26.2 all-gather.2
  93.5 35.1 reduce-scatter.1
where the time goes:
time: 136 us
  blocking collectives  53.9 us (40%)
  waiting for transfers between devices  40.2 us (30%)
  between operations  14.3 us (11%)
  matrix products  9.9 us (7%)
  local copies, waits for them, and re-layouts  9.39 us (7%)
  starting transfers between devices  5.04 us (4%)
  other arithmetic  2.83 us (2%)
    reduce_scatter x1, waiting for transfers between devices, body(): lax.psum_scatter((jnp.dot(attended, output_attend, preferred_element_type...  34.8 us
    all_gather x1, blocking collectives, body(): key_piece = lax.all_gather(expanded, 'sp', axis=0, tiled=True)  16.1 us
    psum x1, blocking collectives, body(): lax.psum(jnp.sum(inputs_f32 * inputs_f32, axis=1, keepdims=True), 'tp')  15.2 us
    all_gather x1, blocking collectives, body(): rope_piece = lax.all_gather(rope_key, 'sp', axis=0, tiled=True)  13.4 us
    all_gather x1, blocking collectives, body(): lax.all_gather(latent_proj.astype(jnp.bfloat16), 'tp', axis=1, tiled=True)  9.26 us
    unnamed x27, local copies, waits for them, and re-layouts  7.86 us
    ppermute x1, starting transfers between devices, with_halo(): before = lax.ppermute(last, axis, up)  3.67 us
    dot_general x1, matrix products, body(): jnp.dot(conv_mixed, output_conv, preferred_element_type=jnp.float32)  3.22 us
  transfers between devices with their start and end apart: 4, of which 3 were waited for; matrix products, arithmetic and copies ran while one was open for 10% of the time, Pallas kernels for 0%

commit v1 on v0

--- a/solution.py
+++ b/solution.py
@@ -79,7 +79,9 @@
         axis=1,
     )
     inputs_f32 = activations.astype(jnp.float32)
-    squares = lax.psum(jnp.sum(inputs_f32 * inputs_f32, axis=1, keepdims=True), "tp")
+    squares = jnp.sum(
+        lax.all_gather(jnp.sum(inputs_f32 * inputs_f32, axis=1, keepdims=True), "tp"), axis=0
+    )
     partial_squares = jnp.zeros((tokens_here, 1), jnp.float32)
     piece_f32 = lax.all_gather(activations, "tp", axis=1, tiled=True).astype(jnp.float32)
     scaled = (piece_f32 * norm_gain).astype(jnp.bfloat16)

time: 136 us -> 136 us (level)
  blocking collectives: 53.9 us -> 49.2 us
  waiting for transfers between devices: 40.2 us -> 44.9 us
    psum x1 -> x0, blocking collectives: 15.2 us -> none  [body(): lax.psum(jnp.sum(inputs_f32 * inputs_f32, axis=1, keepdims=True), 'tp')]
    all_gather x0 -> x1, blocking collectives: none -> 10.4 us  [body(): lax.all_gather(jnp.sum(inputs_f32 * inputs_f32, axis=1, keepdims=True), '...]
    all_gather x1, waiting for transfers between devices: 2.68 us -> 7.34 us  [body(): lax.all_gather(activations, 'tp', axis=1, tiled=True).astype(jnp.float32)]
where the time goes in v1:
time: 136 us; the launch traced here: 135 us
  blocking collectives  49.2 us (36%)
  waiting for transfers between devices  44.9 us (33%)
  between operations  14.3 us (11%)
  matrix products  9.87 us (7%)
  local copies, waits for them, and re-layouts  9.39 us (7%)
  starting transfers between devices  5.05 us (4%)
  other arithmetic  2.86 us (2%)
    reduce_scatter x1, waiting for transfers between devices, body(): lax.psum_scatter((jnp.dot(attended, output_attend, preferred_element_type...  34.8 us
    all_gather x1, blocking collectives, body(): key_piece = lax.all_gather(expanded, 'sp', axis=0, tiled=True)  16.1 us
    all_gather x1, blocking collectives, body(): rope_piece = lax.all_gather(rope_key, 'sp', axis=0, tiled=True)  13.4 us
    all_gather x1, blocking collectives, body(): lax.all_gather(jnp.sum(inputs_f32 * inputs_f32, axis=1, keepdims=True), '...  10.4 us
    all_gather x1, blocking collectives, body(): lax.all_gather(latent_proj.astype(jnp.bfloat16), 'tp', axis=1, tiled=True)  9.25 us
    unnamed x27, local copies, waits for them, and re-layouts  7.86 us
    all_gather x1, waiting for transfers between devices, body(): lax.all_gather(activations, 'tp', axis=1, tiled=True).astype(jnp.float32)  7.34 us
    ppermute x1, starting transfers between devices, with_halo(): before = lax.ppermute(last, axis, up)  3.68 us
  transfers between devices with their start and end apart: 4, of which 3 were waited for; matrix products, arithmetic and copies ran while one was open for 10% of the time, Pallas kernels for 0%

profile of v1, /device:TPU:0, one launch (start us, length us, event | category | flops | bytes accessed | tf_op | source)
XLA Modules:
  0.0 135.5 jit_solution(6472867737686383588)
XLA Ops:
  7.3 0.7 all-gather.5.cloned.1.call-update
  8.0 1.0 multiply_reduce_fusion
  9.0 1.2 copy.19
  10.3 1.3 copy.20
  11.5 1.2 copy.21
  12.8 10.4 %all-gather.2 = f32[8,1,256]{2,1,0:T(1,128)S(1)} all-gather(f32[1,1,256]{2,1,0:T(1,128)S(1)} %bitcast.72), channel_id=2, replica_groups=mesh['sp'=4,'tp'=8] {'tp'}, dimensions={0}, use_global_device_ids=true | all-gather | bytes 9216 | tf_op jit(solution)/shard_map/all_gather | solution.py:83
  23.3 0.6 slice_bitcast_fusion.13
  23.9 0.9 constant_dynamic-update-slice_fusion.5
  24.8 0.7 constant_dynamic-update-slice_fusion.4
  25.6 0.7 constant_dynamic-update-slice_fusion.3
  26.3 0.8 constant_dynamic-update-slice_fusion.2
  27.1 0.9 constant_dynamic-update-slice_fusion.1
  28.0 0.8 constant_dynamic-update-slice_fusion
  28.8 7.3 %all-gather.5.cloned.1.call-done = bf16[256,2048]{1,0:T(8,128)(2,1)} async-done(((bf16[256,256]{1,0:T(8,128)(2,1)}), bf16[256,2048]{1,0:T(8,128)(2,1)}) %all-gather.5.cloned.1.call-update) | async-done | bytes 1048592 | tf_op jit(solution)/shard_map/all_gather | solution.py:86
  36.1 3.1 %convolution_multiply_fusion = f32[256,704]{0,1:T(8,128)S(1)} fusion(bf16[2048,704]{0,1:T(8,128)(2,1)} %constant_dynamic-update-slice_fusion, bf16[256,2048]{1,0:T(8,128)(2,1)} %all-gather.5.cloned.1.call-done, f32[2048]{0:T(1024)S(1)} %copy-done.7, f32[256]{0:T(256)S(1)} %add_rsqrt_fusion.1), kind=kOutput, calls=%fused_computation.6 | convolution fusion | flops 739950592 | bytes 4662272 | tf_op jit(solution)/shard_map/dot_general | solution.py:88
  39.9 13.4 %all-gather.1 = bf16[1024,1,64]{0,2,1:T(8,128)(2,1)S(1)} all-gather(bf16[256,1,64]{0,2,1:T(8,128)(2,1)S(1)} %pad_maximum_fusion), channel_id=3, replica_groups=mesh['sp'=4,'tp'=8] {'sp'}, dimensions={0}, use_global_device_ids=true | all-gather | bytes 163840 | tf_op jit(solution)/shard_map/all_gather | solution.py:128
  53.4 9.3 %all_gather.17 = bf16[256,512]{0,1:T(8,128)(2,1)S(1)} all-gather(bf16[256,64]{0,1:T(8,128)(2,1)S(1)} %slice.196), channel_id=1, replica_groups=mesh['sp'=4,'tp'=8] {'tp'}, dimensions={1}, use_global_device_ids=true | all-gather | bytes 294912 | tf_op jit(solution)/shard_map/all_gather | solution.py:110
  63.2 16.1 %all_gather.18 = bf16[1024,256]{1,0:T(8,128)(2,1)S(1)} all-gather(bf16[256,256]{1,0:T(8,128)(2,1)S(1)} %convolution_convert_fusion), channel_id=1, replica_groups=mesh['sp'=4,'tp'=8] {'sp'}, dimensions={0}, use_global_device_ids=true | all-gather | bytes 655360 | tf_op jit(solution)/shard_map/all_gather | solution.py:127
  80.5 3.7 %collective-permute-start = (bf16[1,128]{0,1:T(8,128)(2,1)S(1)}, bf16[1,128]{0,1:T(8,128)(2,1)S(1)}, u32[]{:S(2)}, u32[]{:S(2)}) collective-permute-start(bf16[1,128]{0,1:T(8,128)(2,1)S(1)} %get-tuple-element.26), channel_id=1, source_target_pairs={{0,8},{8,16},{16,24},{1,9},{9,17},{17,25},{2,10},{10,18},{18,26},{... | collective-permute-start | bytes 776 | tf_op jit(solution)/shard_map/ppermute | solution.py:23
  84.1 1.3 collective-permute-start.1
  85.5 2.4 %fusion.9 = f32[256,2048]{1,0:T(8,128)} fusion(bf16[128,2048]{1,0:T(8,128)(2,1)S(1)} %copy-done, f32[1,256,1024]{2,1,0:T(8,128)S(1)} %get-tuple-element.44, f32[256]{0:T(256)S(1)} %get-tuple-element.43, bf16[1024,1,256]{2,0,1:T(8,128)(2,1)S(1)} %bitcast.69, f32[256]{0:T(256)S(1)} %get-tuple-element.42, f32[256]{0:T(256)S(1)} %get-tuple-element.41), kind=kOutput, calls=%fused_computation.19 | convolution fusion | flops 201949184 | bytes 3935232 | tf_op jit(solution)/shard_map/dot_general | solution.py:166
  87.9 2.1 %collective-permute-done.1 = bf16[1,128]{0,1:T(8,128)(2,1)S(1)} collective-permute-done((bf16[1,128]{0,1:T(8,128)(2,1)S(1)}, bf16[1,128]{0,1:T(8,128)(2,1)S(1)}, u32[]{:S(2)}, u32[]{:S(2)}) %collective-permute-start.1) | collective-permute-done | bytes 288 | tf_op jit(solution)/shard_map/ppermute | solution.py:24
  90.1 3.2 %fusion = bf16[256,2048]{1,0:T(8,128)(2,1)} fusion(f32[256,2048]{1,0:T(8,128)} %fusion.9, bf16[128,2048]{1,0:T(8,128)(2,1)S(1)} %copy-done.2, f32[258,128]{0,1:T(8,128)S(1)} %maximum_convert_fusion, f32[256,704]{0,1:T(8,128)S(1)} %convolution_multiply_fusion, f32[128]{0:T(128)} %get-tuple-element.38, f32[128]{0:T(128)} %get-tuple-element.39, ...), kind=kOutput, calls=%fused_computation.1 | convolution fusion | flops 135495680 | bytes 4195840 | tf_op jit(solution)/shard_map/dot_general | solution.py:167
  93.9 34.8 %reduce-scatter.2.cloned.1.call-done = bf16[32,2048]{1,0:T(8,128)(2,1)} async-done(((bf16[256,2048]{1,0:T(8,128)(2,1)}), bf16[32,2048]{1,0:T(8,128)(2,1)}) %reduce-scatter.2.cloned.1.call-update) | async-done | bytes 131088 | tf_op jit(solution)/shard_map/reduce_scatter | solution.py:164
  (48 shorter events, 3.2 us)
Async XLA Ops:
  7.2 78.3 %copy-start = (bf16[128,2048]{1,0:T(8,128)(2,1)S(1)}, bf16[128,2048]{1,0:T(8,128)(2,1)}, u32[]{:S(2)}) copy-start(bf16[128,2048]{1,0:T(8,128)(2,1)} %param.24) | copy-start | bytes 1572868
  7.2 16.1 %copy-start.5 = (bf16[3,128]{1,0:T(4,128)(2,1)S(1)}, bf16[3,128]{1,0:T(4,128)(2,1)}, u32[]{:S(2)}) copy-start(bf16[3,128]{1,0:T(4,128)(2,1)} %param.23) | copy-start | bytes 2308
  7.2 16.7 %copy-start.1 = (bf16[2048,192]{0,1:T(8,128)(2,1)S(1)}, bf16[2048,192]{0,1:T(8,128)(2,1)}, u32[]{:S(2)}) copy-start(bf16[2048,192]{0,1:T(8,128)(2,1)} %param.15) | copy-start | bytes 2359300
  7.2 17.6 %copy-start.3 = (bf16[2048,64]{0,1:T(8,128)(2,1)S(1)}, bf16[2048,64]{0,1:T(8,128)(2,1)}, u32[]{:S(2)}) copy-start(bf16[2048,64]{0,1:T(8,128)(2,1)} %param.16) | copy-start | bytes 786436
  7.2 18.4 %copy-start.4 = (bf16[2048,64]{0,1:T(8,128)(2,1)S(1)}, bf16[2048,64]{0,1:T(8,128)(2,1)}, u32[]{:S(2)}) copy-start(bf16[2048,64]{0,1:T(8,128)(2,1)} %param.17) | copy-start | bytes 786436
  7.2 28.9 %all-gather.5.cloned.1.call-start = ((), (), s32[]{:S(2)}) async-start(), calls=%async_computation.1 | async-start | bytes 1179648 | tf_op jit(solution)/shard_map/all_gather | solution.py:86
  8.0 120.7 %reduce-scatter.2.cloned.1.call-start = ((), (), s32[]{:S(2)}) async-start(), calls=%async_computation.2 | async-start | bytes 1179648 | tf_op jit(solution)/shard_map/reduce_scatter | solution.py:164
  23.9 12.3 %copy-start.7 = (f32[2048]{0:T(1024)S(1)}, f32[2048]{0:T(1024)}, u32[]{:S(2)}) copy-start(f32[2048]{0:T(1024)} %param.14) | copy-start | bytes 24580
  28.8 34.0 %copy-start.6 = (bf16[512,256]{1,0:T(8,128)(2,1)S(1)}, bf16[512,256]{1,0:T(8,128)(2,1)}, u32[]{:S(2)}) copy-start(bf16[512,256]{1,0:T(8,128)(2,1)} %param.19) | copy-start | bytes 786436
  28.8 34.0 %copy-start.8 = (f32[512]{0:T(512)S(1)}, f32[512]{0:T(512)}, u32[]{:S(2)}) copy-start(f32[512]{0:T(512)} %param.18) | copy-start | bytes 6148
  80.1 10.0 %copy-start.2 = (bf16[128,2048]{1,0:T(8,128)(2,1)S(1)}, bf16[128,2048]{1,0:T(8,128)(2,1)}, u32[]{:S(2)}) copy-start(bf16[128,2048]{1,0:T(8,128)(2,1)} %param.25) | copy-start | bytes 1572868
  80.5 7.4 %collective-permute-start = (bf16[1,128]{0,1:T(8,128)(2,1)S(1)}, bf16[1,128]{0,1:T(8,128)(2,1)S(1)}, u32[]{:S(2)}, u32[]{:S(2)}) collective-permute-start(bf16[1,128]{0,1:T(8,128)(2,1)S(1)} %get-tuple-element.26), channel_id=1, source_target_pairs={{0,8},{8,16},{16,24},{1,9},{9,17},{17,25},{2,10},{10,18},{18,26},{... | collective-permute-start | bytes 776 | tf_op jit(solution)/shard_map/ppermute | solution.py:23
  84.1 5.8 %collective-permute-start.1 = (bf16[1,128]{0,1:T(8,128)(2,1)S(1)}, bf16[1,128]{0,1:T(8,128)(2,1)S(1)}, u32[]{:S(2)}, u32[]{:S(2)}) collective-permute-start(bf16[1,128]{0,1:T(8,128)(2,1)S(1)} %get-tuple-element.36), channel_id=1, source_target_pairs={{8,0},{16,8},{24,16},{9,1},{17,9},{25,17},{10,2},{18,10},{26,18},{... | collective-permute-start | bytes 776 | tf_op jit(solution)/shard_map/ppermute | solution.py:24
Sparse Core Ops, SparseCore 0:
  9.9 26.1 all-gather.4
  93.4 35.1 reduce-scatter.1
